TPU v7x, 32 devices: a whole 2x2x4 slice. The times are simulated.
32 devices in a mesh: kv: 8 (over z, core), tp: 4 (over y, x).
Axes of the slice: x: 2, y: 2, z: 4, core: 2. Of those that a mesh axis runs over, the one named last changes fastest.
Arguments:
- tokens: bfloat16 [16, 2048], P(None, 'kv'), may hold values from -8 to 8
- lengths: int32 [16], replicated, may hold values from 1 to 3072, 12288 in all
- latent_cache: bfloat16 [16, 3072, 256], P(None, ('kv', 'tp')), may hold values from -10 to 10
- rope_cache: bfloat16 [16, 3072, 32], P(None, ('kv', 'tp')), may hold values from -2000 to 2000
- gain_in: bfloat16 [2048], P('kv'), may hold values from 0.099609375 to 1.8984375
- w_down_q: bfloat16 [2048, 512], P('kv'), may hold values from -0.125 to 0.125
- w_down_kv: bfloat16 [2048, 256], P('kv'), may hold values from -0.125 to 0.125
- w_rope_key: bfloat16 [2048, 32], P('kv'), may hold values from -0.125 to 0.125
- gain_q: bfloat16 [512], replicated, may hold values from 0.099609375 to 1.8984375
- w_up_qn: bfloat16 [512, 16, 64], replicated, may hold values from -0.25 to 0.25
- w_up_qr: bfloat16 [512, 16, 32], replicated, may hold values from -0.25 to 0.25
- gain_kv: bfloat16 [256], replicated, may hold values from 0.099609375 to 1.8984375
- w_key_up: bfloat16 [256, 16, 64], replicated, may hold values from -0.375 to 0.375
- w_value_up: bfloat16 [256, 16, 64], replicated, may hold values from -0.375 to 0.375
- w_attn_out: bfloat16 [16, 64, 2048], P('tp', None, 'kv'), may hold values from -0.1875 to 0.1875
- gain_mid: bfloat16 [2048], P('kv'), may hold values from 0.099609375 to 1.8984375
- w_ff_in: bfloat16 [2048, 8192], P('kv', 'tp'), may hold values from -0.125 to 0.125
- w_ff_out: bfloat16 [8192, 2048], P('tp', 'kv'), may hold values from -0.0625 to 0.0625
Outputs:
- mixed: bfloat16 [16, 2048], P(None, 'kv')
- new_latent: bfloat16 [16, 256], replicated
- new_rope_key: bfloat16 [16, 32], replicated
Inputs may be any that keep to these rules, and one draw needn't show every extreme that they name: `lengths`: each sequence's live cache positions; one sequence fills the whole cache.
All inputs are finite; a program needn't handle non-finite values.
Results may differ from a plain program's by a relative error of at most 0.012.
Values sent between devices are 32-bit elements; how exact they have to be, the bound alone decides.
No kernel may reach another device: no remote copies, remote signals or barrier semaphores. Data moves between devices by JAX's collectives and lax.ppermute only.
A program may use at most 64 MiB of HBM per device.

v0:
```python
import jax
import jax.numpy as jnp
from jax import lax
from jax.sharding import PartitionSpec as P

D = 2048
NOPE = 64
ROPE = 32
EPS = 1e-06


def combined_all(part, axis, combine):
    gathered = jax.tree.map(lambda a: lax.all_gather(a, axis), part)

    def take(source):
        return jax.tree.map(lambda a: lax.dynamic_index_in_dim(a, source, 0, False), gathered)

    return lax.fori_loop(
        1, lax.axis_size(axis), lambda source, state: combine(state, take(source)), take(0)
    )


def rotate(values, positions):
    half = values.shape[-1] // 2
    inverse = 10000.0 ** (-jnp.arange(half, dtype=jnp.float32) / half)
    angle = positions.astype(jnp.float32)[:, None, None] * inverse[None, None, :]
    first = values[..., :half]
    second = values[..., half:]
    return jnp.concatenate(
        [
            first * jnp.cos(angle) - second * jnp.sin(angle),
            second * jnp.cos(angle) + first * jnp.sin(angle),
        ],
        axis=-1,
    )


def rms_scaled(values, gain):
    return (
        values
        * lax.rsqrt(jnp.mean(values * values, axis=-1, keepdims=True) + EPS)
        * gain.astype(jnp.float32)
    )


def combine(earlier, later):
    top_a, total_a, acc_a = earlier
    top_b, total_b, acc_b = later
    top = jnp.maximum(top_a, top_b)
    fade_a = jnp.exp(top_a - top)
    fade_b = jnp.exp(top_b - top)
    return (
        top,
        total_a * fade_a + total_b * fade_b,
        acc_a * fade_a[..., None] + acc_b * fade_b[..., None],
    )


def fold_sources(parts):
    tops, totals, accs = parts
    top = jnp.max(tops, axis=0)
    fade = jnp.exp(tops - top[None])
    return (top, jnp.sum(totals * fade, axis=0), jnp.sum(accs * fade[..., None], axis=0))


def per_device(
    tokens,
    lengths,
    latent_cache,
    rope_cache,
    gain_in,
    w_down_q,
    w_down_kv,
    w_rope_key,
    gain_q,
    w_up_qn,
    w_up_qr,
    gain_kv,
    w_key_up,
    w_value_up,
    w_attn_out,
    gain_mid,
    w_ff_in,
    w_ff_out,
):
    f32 = jnp.float32
    bf16 = jnp.bfloat16
    highest = lax.Precision.HIGHEST
    scale = (NOPE + ROPE) ** (-0.5)
    resid = tokens.astype(f32)
    scaled_in = (resid * gain_in.astype(f32)).astype(bf16)
    part_q = jnp.dot(scaled_in, w_down_q, preferred_element_type=f32)
    part_kv = jnp.dot(scaled_in, w_down_kv, preferred_element_type=f32)
    part_rope = jnp.dot(scaled_in, w_rope_key, preferred_element_type=f32)
    square_in = jnp.sum(resid * resid, axis=1)
    sum_q, sum_kv, sum_rope, total_in = lax.psum((part_q, part_kv, part_rope, square_in), "kv")
    inv_in = lax.rsqrt(total_in / D + EPS)[:, None]
    query_latent = rms_scaled(inv_in * sum_q, gain_q).astype(bf16)
    new_latent = rms_scaled(inv_in * sum_kv, gain_kv).astype(bf16)
    new_rope_key = rotate((inv_in * sum_rope)[:, None, :], lengths)[:, 0, :].astype(bf16)
    query_nope = jnp.einsum(
        "bc,chd->bhd", query_latent, w_up_qn, preferred_element_type=f32
    ).astype(bf16)
    query_rope = rotate(
        jnp.einsum("bc,chr->bhr", query_latent, w_up_qr, preferred_element_type=f32), lengths
    ).astype(bf16)
    query_cache = jnp.einsum(
        "bhd,khd->bhk", query_nope, w_key_up, preferred_element_type=f32
    ).astype(bf16)
    rows = latent_cache.shape[1]
    positions = lax.axis_index(("kv", "tp")) * rows + jnp.arange(rows, dtype=jnp.int32)
    live = (positions[None, :] < lengths[:, None])[:, None, :]
    scores = (
        jnp.einsum("bhk,blk->bhl", query_cache, latent_cache, preferred_element_type=f32)
        + jnp.einsum("bhr,blr->bhl", query_rope, rope_cache, preferred_element_type=f32)
    ) * scale
    scores = jnp.where(live, scores, -1e30)
    top = jnp.max(scores, axis=2)
    weights = jnp.where(live, jnp.exp(scores - top[:, :, None]), 0.0)
    total = jnp.sum(weights, axis=2)
    acc = jnp.einsum("bhl,blk->bhk", weights.astype(bf16), latent_cache, preferred_element_type=f32)
    heads_dev = w_attn_out.shape[0]
    first_head = lax.axis_index("tp") * heads_dev
    own_value_up = lax.dynamic_slice_in_dim(w_value_up, first_head, heads_dev, 1).astype(f32)
    own_cache_q = lax.dynamic_slice_in_dim(query_cache, first_head, heads_dev, 1)
    own_rope_q = lax.dynamic_slice_in_dim(query_rope, first_head, heads_dev, 1)
    self_score = (
        jnp.einsum("bhk,bk->bh", own_cache_q, new_latent, preferred_element_type=f32)
        + jnp.einsum("bhr,br->bh", own_rope_q, new_rope_key, preferred_element_type=f32)
    ) * scale
    top, total, acc = fold_sources(
        (
            lax.all_to_all(top[None], "tp", split_axis=2, concat_axis=0, tiled=True),
            lax.all_to_all(total[None], "tp", split_axis=2, concat_axis=0, tiled=True),
            lax.all_to_all(acc[None], "tp", split_axis=2, concat_axis=0, tiled=True),
        )
    )
    top, total, acc = combined_all((top, total, acc), "kv", combine)
    joined = jnp.maximum(top, self_score)
    fade = jnp.exp(top - joined)
    self_weight = jnp.exp(self_score - joined)
    total = total * fade + self_weight
    acc = (
        acc * fade[:, :, None]
        + self_weight.astype(bf16).astype(f32)[:, :, None] * new_latent.astype(f32)[:, None, :]
    )
    expanded = jnp.einsum("bhk,khv->bhv", acc, own_value_up, precision=highest)
    head_out = (expanded / total[:, :, None]).astype(bf16)
    attn_part = jnp.einsum("bhv,hvd->bd", head_out, w_attn_out, preferred_element_type=f32)
    resid_mid = resid + lax.psum(attn_part, "tp")
    scaled_mid = (resid_mid * gain_mid.astype(f32)).astype(bf16)
    hidden_part = jnp.dot(scaled_mid, w_ff_in, preferred_element_type=f32)
    square_mid = jnp.sum(resid_mid * resid_mid, axis=1)
    hidden_sum, total_mid = lax.psum((hidden_part, square_mid), "kv")
    inv_mid = lax.rsqrt(total_mid / D + EPS)[:, None]
    hidden = jnp.square(jax.nn.relu(inv_mid * hidden_sum)).astype(bf16)
    out_part = jnp.dot(hidden, w_ff_out, preferred_element_type=f32)
    mixed = (resid_mid + lax.psum(out_part, "tp")).astype(bf16)
    return (mixed, new_latent, new_rope_key)


def solution(mesh):
    return jax.shard_map(
        per_device,
        mesh=mesh,
        in_specs=(
            P(None, "kv"),
            P(),
            P(None, ("kv", "tp"), None),
            P(None, ("kv", "tp"), None),
            P("kv"),
            P("kv", None),
            P("kv", None),
            P("kv", None),
            P(),
            P(),
            P(),
            P(),
            P(),
            P(),
            P("tp", None, "kv"),
            P("kv"),
            P("kv", "tp"),
            P("tp", "kv"),
        ),
        out_specs=(P(None, "kv"), P(), P()),
        check_vma=False,
    )
```

profile of v0, /device:TPU:0, one launch (start us, length us, event | category | flops | bytes accessed | tf_op | source)
XLA Modules:
  0.0 218.2 jit_solution(16655276583001931939)
XLA Ops:
  7.2 0.8 convert_element_type.75
  8.0 0.8 fusion.23
  8.8 0.7 convert_element_type.68
  9.5 0.7 broadcast_compare_fusion
  10.2 0.7 convert_element_type.70
  10.9 0.9 fusion.41
  11.7 1.1 fusion.43
  12.8 1.2 fusion.45
  14.0 30.8 %all-reduce = (f32[16,512]{1,0:T(8,128)S(1)}, f32[16]{0:T(128)S(1)}, f32[16,256]{1,0:T(8,128)S(1)}, f32[16,32]{1,0:T(8,128)S(1)}) all-reduce(f32[16,512]{1,0:T(8,128)S(1)} %fusion.45, f32[16]{0:T(128)S(1)} %fusion.23, f32[16,256]{1,0:T(8,128)S(1)} %fusion.43, f32[16,32]{1,0:T(8,128)S(1)} %fusion.41), channel_id=1, replica_groups=mesh['kv'=8,'tp'=4] {'kv'}, use_global_device_ids=true, to_apply=%region_2.0 | all-reduce | flops 12816 | bytes 102528 | tf_op jit(solution)/shard_map/psum | solution.py:96
  45.6 0.7 convolution_convert_fusion
  46.7 0.8 copy-done.1
  47.8 0.7 copy.50
  48.5 3.7 %all-to-all-start = ((f32[1,16,16]{1,0,2:T(1,128)}), f32[1,16,16]{1,0,2:T(1,128)S(1)}, u32[]{:S(2)}, u32[]{:S(2)}) async-start(f32[1,16,16]{1,0,2:T(1,128)} %copy.50), calls=%async_computation | async-start | bytes 16384 | tf_op jit(solution)/shard_map/all_to_all | solution.py:133
  52.3 0.6 copy-done.10
  53.6 0.7 fusion.52
  55.3 0.6 copy-done.11
  56.1 0.7 copy.51
  56.8 0.8 copy.52
  57.6 4.2 %all-to-all-start.1 = ((f32[1,16,16]{1,0,2:T(1,128)}), f32[1,16,16]{1,0,2:T(1,128)S(1)}, u32[]{:S(2)}, u32[]{:S(2)}) async-start(f32[1,16,16]{1,0,2:T(1,128)} %copy.51), calls=%async_computation.1 | async-start | bytes 16384 | tf_op jit(solution)/shard_map/all_to_all | solution.py:134
  61.8 12.8 %all-gather.3 = f32[8,16,4]{1,2,0:T(4,128)S(1)} all-gather(f32[1,16,4]{1,2,0:T(4,128)S(1)} %bitcast.113), channel_id=2, replica_groups=mesh['kv'=8,'tp'=4] {'kv'}, dimensions={0}, use_global_device_ids=true | all-gather | bytes 2304 | tf_op jit(solution)/shard_map/all_gather | solution.py:13
  74.6 4.2 %all-to-all-start.2 = ((f32[1,16,16,256]{3,1,0,2:T(8,128)}), f32[1,16,16,256]{3,1,0,2:T(8,128)S(1)}, u32[]{:S(2)}, u32[]{:S(2)}) async-start(f32[1,16,16,256]{3,1,0,2:T(8,128)} %copy.52), calls=%async_computation.2 | async-start | bytes 524288 | tf_op jit(solution)/shard_map/all_to_all | solution.py:135
  78.8 12.8 %all-gather.4 = f32[8,16,4]{1,2,0:T(4,128)S(1)} all-gather(f32[1,16,4]{1,2,0:T(4,128)S(1)} %bitcast.114), channel_id=3, replica_groups=mesh['kv'=8,'tp'=4] {'kv'}, dimensions={0}, use_global_device_ids=true | all-gather | bytes 2304 | tf_op jit(solution)/shard_map/all_gather | solution.py:13
  91.8 15.1 %all-gather.2 = f32[128,4,256]{2,1,0:T(4,128)S(1)} all-gather(f32[16,4,256]{2,1,0:T(4,128)S(1)} %copy.53), channel_id=4, replica_groups=mesh['kv'=8,'tp'=4] {'kv'}, dimensions={0}, use_global_device_ids=true | all-gather | bytes 589824 | tf_op jit(solution)/shard_map/all_gather | solution.py:13
  106.8 2.5 %while.19 = (s32[]{:T(128)}, f32[16,4]{0,1:T(4,128)S(1)}, f32[16,4]{0,1:T(4,128)S(1)}, f32[16,4,256]{2,1,0:T(4,128)S(1)}, f32[8,16,4]{1,2,0:T(4,128)S(1)}, /*ind...) while((s32[]{:T(128)}, f32[16,4]{0,1:T(4,128)S(1)}, ...), condition=%wide.region_10.11_spmd, body=%wide.region_9.10_spmd.sunk | while | flops 49541 | bytes 200335 | solution.py:18
  109.6 1.2 fusion.6
  111.0 16.5 %psum.60 = f32[16,256]{1,0:T(8,128)S(1)} all-reduce(f32[16,256]{1,0:T(8,128)S(1)} %convolution_bitcast_fusion.2), channel_id=1, replica_groups=mesh['kv'=8,'tp'=4] {'tp'}, use_global_device_ids=true, to_apply=%region_14.15 | all-reduce | flops 4096 | bytes 32768 | tf_op jit(solution)/shard_map/psum | solution.py:150
  127.6 13.6 %psum.61 = f32[16]{0:T(128)S(1)} all-reduce(f32[16]{0:T(128)S(1)} %multiply_reduce_fusion.2), channel_id=1, replica_groups=mesh['kv'=8,'tp'=4] {'kv'}, use_global_device_ids=true, to_apply=%region_16.17 | all-reduce | flops 16 | bytes 128 | tf_op jit(solution)/shard_map/psum | solution.py:154
  141.2 0.9 fusion.38
  142.2 51.4 %all-reduce.3.cloned.1.call-done = f32[16,2048]{1,0:T(8,128)} async-done(((f32[16,2048]{1,0:T(8,128)}), f32[16,2048]{1,0:T(8,128)}) %all-reduce.3.cloned.1.call-update) | async-done | bytes 131088 | tf_op jit(solution)/shard_map/psum | solution.py:154
  193.6 1.2 fusion.12
  194.8 16.0 %psum.63 = f32[16,256]{1,0:T(8,128)S(1)} all-reduce(f32[16,256]{1,0:T(8,128)S(1)} %fusion.12), channel_id=1, replica_groups=mesh['kv'=8,'tp'=4] {'tp'}, use_global_device_ids=true, to_apply=%region_18.19 | all-reduce | flops 4096 | bytes 32768 | tf_op jit(solution)/shard_map/psum | solution.py:158
  210.7 0.6 add_convert_fusion.1
  (94 shorter events, 6.7 us)
Async XLA Ops:
  7.2 38.4 %copy-start = (bf16[512,16,64]{0,2,1:T(8,128)(2,1)S(1)}, bf16[512,16,64]{0,2,1:T(8,128)(2,1)}, u32[]{:S(2)}) copy-start(bf16[512,16,64]{0,2,1:T(8,128)(2,1)} %param.29) | copy-start | bytes 3145732
  7.2 37.9 %copy-start.4 = (bf16[512,16,32]{0,2,1:T(8,128)(2,1)S(1)}, bf16[512,16,32]{0,2,1:T(8,128)(2,1)}, u32[]{:S(2)}) copy-start(bf16[512,16,32]{0,2,1:T(8,128)(2,1)} %param.30) | copy-start | bytes 1572868
  12.8 32.8 %copy-start.5 = (bf16[256,16,64]{0,2,1:T(8,128)(2,1)S(1)}, bf16[256,16,64]{0,2,1:T(8,128)(2,1)}, u32[]{:S(2)}) copy-start(bf16[256,16,64]{0,2,1:T(8,128)(2,1)} %param.32) | copy-start | bytes 1572868
  45.6 0.9 copy-start.8
  46.3 1.2 copy-start.1
  48.5 9.1 %all-to-all-start = ((f32[1,16,16]{1,0,2:T(1,128)}), f32[1,16,16]{1,0,2:T(1,128)S(1)}, u32[]{:S(2)}, u32[]{:S(2)}) async-start(f32[1,16,16]{1,0,2:T(1,128)} %copy.50), calls=%async_computation | async-start | bytes 16384 | tf_op jit(solution)/shard_map/all_to_all | solution.py:133
  52.2 0.7 copy-start.10
  54.3 0.6 copy-start.9
  55.3 0.7 copy-start.11
  57.6 17.0 %all-to-all-start.1 = ((f32[1,16,16]{1,0,2:T(1,128)}), f32[1,16,16]{1,0,2:T(1,128)S(1)}, u32[]{:S(2)}, u32[]{:S(2)}) async-start(f32[1,16,16]{1,0,2:T(1,128)} %copy.51), calls=%async_computation.1 | async-start | bytes 16384 | tf_op jit(solution)/shard_map/all_to_all | solution.py:134
  74.6 17.0 %all-to-all-start.2 = ((f32[1,16,16,256]{3,1,0,2:T(8,128)}), f32[1,16,16,256]{3,1,0,2:T(8,128)S(1)}, u32[]{:S(2)}, u32[]{:S(2)}) async-start(f32[1,16,16,256]{3,1,0,2:T(8,128)} %copy.52), calls=%async_computation.2 | async-start | bytes 524288 | tf_op jit(solution)/shard_map/all_to_all | solution.py:135
  78.8 114.8 %all-reduce.3.cloned.1.call-start = ((), (), s32[]{:S(2)}) async-start(), calls=%async_computation.3 | async-start | bytes 262144 | tf_op jit(solution)/shard_map/psum | solution.py:154
  91.7 19.0 %copy-start.7 = (bf16[4,64,256]{2,1,0:T(8,128)(2,1)S(1)}, bf16[4,64,256]{2,1,0:T(8,128)(2,1)}, u32[]{:S(2)}) copy-start(bf16[4,64,256]{2,1,0:T(8,128)(2,1)} %param.34) | copy-start | bytes 393220
  106.8 34.4 %copy-start.2 = (bf16[256,2048]{1,0:T(8,128)(2,1)S(1)}, bf16[256,2048]{1,0:T(8,128)(2,1)}, u32[]{:S(2)}) copy-start(bf16[256,2048]{1,0:T(8,128)(2,1)} %param.36) | copy-start | bytes 3145732
  106.8 20.7 %copy-start.6 = (bf16[16,256]{1,0:T(8,128)(2,1)S(1)}, bf16[16,256]{1,0:T(8,128)(2,1)}, u32[]{:S(2)}) copy-start(bf16[16,256]{1,0:T(8,128)(2,1)} %param.20) | copy-start | bytes 24580
  109.3 84.3 %copy-start.3 = (bf16[2048,256]{1,0:T(8,128)(2,1)S(1)}, bf16[2048,256]{1,0:T(8,128)(2,1)}, u32[]{:S(2)}) copy-start(bf16[2048,256]{1,0:T(8,128)(2,1)} %param.37) | copy-start | bytes 3145732
Sparse Core Ops, SparseCore 0:
  142.3 51.2 all-reduce.2
where the time goes:
time: 219 us; the launch traced here: 218 us
  blocking collectives  117 us (53%)
  waiting for transfers between devices  51.5 us (24%)
  between operations  14.2 us (6%)
  starting transfers between devices  12.1 us (6%)
  matrix products  8.74 us (4%)
  other arithmetic  7.81 us (4%)
  local copies, waits for them, and re-layouts  6.26 us (3%)
    psum x1, waiting for transfers between devices, per_device(): hidden_sum, total_mid = lax.psum((hidden_part, square_mid), 'kv')  51.4 us
    all_gather x3, blocking collectives, combined_all(): gathered = jax.tree.map(lambda a: lax.all_gather(a, axis), part)  40.6 us
    psum x1, blocking collectives, per_device(): lax.psum((part_q, part_kv, part_rope, square_in), 'kv')  30.8 us
    psum x1, blocking collectives, per_device(): resid_mid = resid + lax.psum(attn_part, 'tp')  16.5 us
    psum x1, blocking collectives, per_device(): mixed = (resid_mid + lax.psum(out_part, 'tp')).astype(bf16)  16 us
    psum x1, blocking collectives, per_device(): hidden_sum, total_mid = lax.psum((hidden_part, square_mid), 'kv')  13.6 us
  transfers between devices with their start and end apart: 4, of which 1 were waited for; matrix products, arithmetic and copies ran while one was open for 2% of the time, Pallas kernels for 0%

commit v1 on v0

--- a/solution.py
+++ b/solution.py
@@ -147,7 +147,7 @@
     expanded = jnp.einsum("bhk,khv->bhv", acc, own_value_up, precision=highest)
     head_out = (expanded / total[:, :, None]).astype(bf16)
     attn_part = jnp.einsum("bhv,hvd->bd", head_out, w_attn_out, preferred_element_type=f32)
-    resid_mid = resid + lax.psum(attn_part, "tp")
+    resid_mid = resid + jnp.sum(lax.all_gather(attn_part, "tp"), axis=0)
     scaled_mid = (resid_mid * gain_mid.astype(f32)).astype(bf16)
     hidden_part = jnp.dot(scaled_mid, w_ff_in, preferred_element_type=f32)
     square_mid = jnp.sum(resid_mid * resid_mid, axis=1)

time: 219 us -> 212 us (0.968)
  blocking collectives: 117 us -> 110 us
    psum x1 -> x0, blocking collectives: 16.5 us -> none  [per_device(): resid_mid = resid + lax.psum(attn_part, 'tp')]
    all_gather x0 -> x1, blocking collectives: none -> 8.75 us  [per_device(): resid_mid = resid + jnp.sum(lax.all_gather(attn_part, 'tp'), axis=0)]
where the time goes in v1:
time: 212 us; the launch traced here: 211 us
  blocking collectives  110 us (52%)
  waiting for transfers between devices  52.4 us (25%)
  between operations  14.3 us (7%)
  starting transfers between devices  12.1 us (6%)
  matrix products  8.78 us (4%)
  other arithmetic  7.82 us (4%)
  local copies, waits for them, and re-layouts  6.25 us (3%)
    psum x1, waiting for transfers between devices, per_device(): hidden_sum, total_mid = lax.psum((hidden_part, square_mid), 'kv')  52.3 us
    all_gather x3, blocking collectives, combined_all(): gathered = jax.tree.map(lambda a: lax.all_gather(a, axis), part)  40.5 us
    psum x1, blocking collectives, per_device(): lax.psum((part_q, part_kv, part_rope, square_in), 'kv')  30.8 us
    psum x1, blocking collectives, per_device(): mixed = (resid_mid + lax.psum(out_part, 'tp')).astype(bf16)  16 us
    psum x1, blocking collectives, per_device(): hidden_sum, total_mid = lax.psum((hidden_part, square_mid), 'kv')  13.6 us
    all_gather x1, blocking collectives, per_device(): resid_mid = resid + jnp.sum(lax.all_gather(attn_part, 'tp'), axis=0)  8.75 us
  transfers between devices with their start and end apart: 4, of which 1 were waited for; matrix products, arithmetic and copies ran while one was open for 2% of the time, Pallas kernels for 0%

profile of v1, /device:TPU:0, one launch (start us, length us, event | category | flops | bytes accessed | tf_op | source)
XLA Modules:
  0.0 211.3 jit_solution(5430203213944652060)
XLA Ops:
  7.2 0.8 convert_element_type.75
  8.0 0.8 fusion.23
  8.8 0.7 convert_element_type.68
  9.5 0.7 broadcast_compare_fusion
  10.2 0.7 convert_element_type.70
  10.9 0.9 fusion.41
  11.7 1.1 fusion.43
  12.8 1.2 fusion.45
  14.0 30.8 %all-reduce = (f32[16,512]{1,0:T(8,128)S(1)}, f32[16]{0:T(128)S(1)}, f32[16,256]{1,0:T(8,128)S(1)}, f32[16,32]{1,0:T(8,128)S(1)}) all-reduce(f32[16,512]{1,0:T(8,128)S(1)} %fusion.45, f32[16]{0:T(128)S(1)} %fusion.23, f32[16,256]{1,0:T(8,128)S(1)} %fusion.43, f32[16,32]{1,0:T(8,128)S(1)} %fusion.41), channel_id=1, replica_groups=mesh['kv'=8,'tp'=4] {'kv'}, use_global_device_ids=true, to_apply=%region_2.0 | all-reduce | flops 12816 | bytes 102528 | tf_op jit(solution)/shard_map/psum | solution.py:96
  45.6 0.7 convolution_convert_fusion
  46.7 0.8 copy-done.1
  47.8 0.7 copy.50
  48.5 3.7 %all-to-all-start = ((f32[1,16,16]{1,0,2:T(1,128)}), f32[1,16,16]{1,0,2:T(1,128)S(1)}, u32[]{:S(2)}, u32[]{:S(2)}) async-start(f32[1,16,16]{1,0,2:T(1,128)} %copy.50), calls=%async_computation | async-start | bytes 16384 | tf_op jit(solution)/shard_map/all_to_all | solution.py:133
  52.3 0.6 copy-done.10
  53.6 0.7 fusion.52
  55.3 0.6 copy-done.11
  56.1 0.7 copy.51
  56.8 0.8 copy.52
  57.6 4.2 %all-to-all-start.1 = ((f32[1,16,16]{1,0,2:T(1,128)}), f32[1,16,16]{1,0,2:T(1,128)S(1)}, u32[]{:S(2)}, u32[]{:S(2)}) async-start(f32[1,16,16]{1,0,2:T(1,128)} %copy.51), calls=%async_computation.1 | async-start | bytes 16384 | tf_op jit(solution)/shard_map/all_to_all | solution.py:134
  61.8 12.8 %all-gather.4 = f32[8,16,4]{1,2,0:T(4,128)S(1)} all-gather(f32[1,16,4]{1,2,0:T(4,128)S(1)} %bitcast.115), channel_id=2, replica_groups=mesh['kv'=8,'tp'=4] {'kv'}, dimensions={0}, use_global_device_ids=true | all-gather | bytes 2304 | tf_op jit(solution)/shard_map/all_gather | solution.py:13
  74.6 4.2 %all-to-all-start.2 = ((f32[1,16,16,256]{3,1,0,2:T(8,128)}), f32[1,16,16,256]{3,1,0,2:T(8,128)S(1)}, u32[]{:S(2)}, u32[]{:S(2)}) async-start(f32[1,16,16,256]{3,1,0,2:T(8,128)} %copy.52), calls=%async_computation.2 | async-start | bytes 524288 | tf_op jit(solution)/shard_map/all_to_all | solution.py:135
  78.8 12.8 %all-gather.5 = f32[8,16,4]{1,2,0:T(4,128)S(1)} all-gather(f32[1,16,4]{1,2,0:T(4,128)S(1)} %bitcast.116), channel_id=3, replica_groups=mesh['kv'=8,'tp'=4] {'kv'}, dimensions={0}, use_global_device_ids=true | all-gather | bytes 2304 | tf_op jit(solution)/shard_map/all_gather | solution.py:13
  91.7 14.9 %all-gather.2 = f32[128,4,256]{2,1,0:T(4,128)S(1)} all-gather(f32[16,4,256]{2,1,0:T(4,128)S(1)} %copy.53), channel_id=4, replica_groups=mesh['kv'=8,'tp'=4] {'kv'}, dimensions={0}, use_global_device_ids=true | all-gather | bytes 589824 | tf_op jit(solution)/shard_map/all_gather | solution.py:13
  106.7 2.5 %while.19 = (s32[]{:T(128)}, f32[16,4]{0,1:T(4,128)S(1)}, f32[16,4]{0,1:T(4,128)S(1)}, f32[16,4,256]{2,1,0:T(4,128)S(1)}, f32[8,16,4]{1,2,0:T(4,128)S(1)}, /*ind...) while((s32[]{:T(128)}, f32[16,4]{0,1:T(4,128)S(1)}, ...), condition=%wide.region_10.11_spmd, body=%wide.region_9.10_spmd.sunk | while | flops 49541 | bytes 200335 | solution.py:18
  109.5 1.2 fusion.6
  110.9 8.7 %all-gather.3 = f32[64,256]{1,0:T(8,128)S(1)} all-gather(f32[16,256]{1,0:T(8,128)S(1)} %convolution_bitcast_fusion.2), channel_id=5, replica_groups=mesh['kv'=8,'tp'=4] {'tp'}, dimensions={0}, use_global_device_ids=true | all-gather | bytes 81920 | tf_op jit(solution)/shard_map/all_gather | solution.py:150
  119.8 13.6 %psum.53 = f32[16]{0:T(128)S(1)} all-reduce(f32[16]{0:T(128)S(1)} %multiply_reduce_fusion.2), channel_id=1, replica_groups=mesh['kv'=8,'tp'=4] {'kv'}, use_global_device_ids=true, to_apply=%region_16.17 | all-reduce | flops 16 | bytes 128 | tf_op jit(solution)/shard_map/psum | solution.py:154
  133.4 0.9 fusion.38
  134.3 52.3 %all-reduce.3.cloned.1.call-done = f32[16,2048]{1,0:T(8,128)} async-done(((f32[16,2048]{1,0:T(8,128)}), f32[16,2048]{1,0:T(8,128)}) %all-reduce.3.cloned.1.call-update) | async-done | bytes 131088 | tf_op jit(solution)/shard_map/psum | solution.py:154
  186.6 1.2 fusion.12
  187.8 16.0 %psum.55 = f32[16,256]{1,0:T(8,128)S(1)} all-reduce(f32[16,256]{1,0:T(8,128)S(1)} %fusion.12), channel_id=1, replica_groups=mesh['kv'=8,'tp'=4] {'tp'}, use_global_device_ids=true, to_apply=%region_18.19 | all-reduce | flops 4096 | bytes 32768 | tf_op jit(solution)/shard_map/psum | solution.py:158
  203.8 0.6 add_convert_fusion.1
  (95 shorter events, 6.7 us)
Async XLA Ops:
  7.2 38.4 %copy-start = (bf16[512,16,64]{0,2,1:T(8,128)(2,1)S(1)}, bf16[512,16,64]{0,2,1:T(8,128)(2,1)}, u32[]{:S(2)}) copy-start(bf16[512,16,64]{0,2,1:T(8,128)(2,1)} %param.29) | copy-start | bytes 3145732
  7.2 37.9 %copy-start.4 = (bf16[512,16,32]{0,2,1:T(8,128)(2,1)S(1)}, bf16[512,16,32]{0,2,1:T(8,128)(2,1)}, u32[]{:S(2)}) copy-start(bf16[512,16,32]{0,2,1:T(8,128)(2,1)} %param.30) | copy-start | bytes 1572868
  12.8 32.8 %copy-start.5 = (bf16[256,16,64]{0,2,1:T(8,128)(2,1)S(1)}, bf16[256,16,64]{0,2,1:T(8,128)(2,1)}, u32[]{:S(2)}) copy-start(bf16[256,16,64]{0,2,1:T(8,128)(2,1)} %param.32) | copy-start | bytes 1572868
  45.6 0.9 copy-start.8
  46.3 1.2 copy-start.1
  48.5 9.1 %all-to-all-start = ((f32[1,16,16]{1,0,2:T(1,128)}), f32[1,16,16]{1,0,2:T(1,128)S(1)}, u32[]{:S(2)}, u32[]{:S(2)}) async-start(f32[1,16,16]{1,0,2:T(1,128)} %copy.50), calls=%async_computation | async-start | bytes 16384 | tf_op jit(solution)/shard_map/all_to_all | solution.py:133
  52.2 0.7 copy-start.10
  54.3 0.6 copy-start.9
  55.3 0.7 copy-start.11
  57.6 17.0 %all-to-all-start.1 = ((f32[1,16,16]{1,0,2:T(1,128)}), f32[1,16,16]{1,0,2:T(1,128)S(1)}, u32[]{:S(2)}, u32[]{:S(2)}) async-start(f32[1,16,16]{1,0,2:T(1,128)} %copy.51), calls=%async_computation.1 | async-start | bytes 16384 | tf_op jit(solution)/shard_map/all_to_all | solution.py:134
  74.6 17.0 %all-to-all-start.2 = ((f32[1,16,16,256]{3,1,0,2:T(8,128)}), f32[1,16,16,256]{3,1,0,2:T(8,128)S(1)}, u32[]{:S(2)}, u32[]{:S(2)}) async-start(f32[1,16,16,256]{3,1,0,2:T(8,128)} %copy.52), calls=%async_computation.2 | async-start | bytes 524288 | tf_op jit(solution)/shard_map/all_to_all | solution.py:135
  78.8 107.8 %all-reduce.3.cloned.1.call-start = ((), (), s32[]{:S(2)}) async-start(), calls=%async_computation.3 | async-start | bytes 262144 | tf_op jit(solution)/shard_map/psum | solution.py:154
  106.7 4.0 %copy-start.7 = (bf16[4,64,256]{2,1,0:T(8,128)(2,1)S(1)}, bf16[4,64,256]{2,1,0:T(8,128)(2,1)}, u32[]{:S(2)}) copy-start(bf16[4,64,256]{2,1,0:T(8,128)(2,1)} %param.34) | copy-start | bytes 393220
  106.7 13.0 %copy-start.6 = (bf16[16,256]{1,0:T(8,128)(2,1)S(1)}, bf16[16,256]{1,0:T(8,128)(2,1)}, u32[]{:S(2)}) copy-start(bf16[16,256]{1,0:T(8,128)(2,1)} %param.20) | copy-start | bytes 24580
  106.7 26.7 %copy-start.2 = (bf16[256,2048]{1,0:T(8,128)(2,1)S(1)}, bf16[256,2048]{1,0:T(8,128)(2,1)}, u32[]{:S(2)}) copy-start(bf16[256,2048]{1,0:T(8,128)(2,1)} %param.36) | copy-start | bytes 3145732
  109.4 77.3 %copy-start.3 = (bf16[2048,256]{1,0:T(8,128)(2,1)S(1)}, bf16[2048,256]{1,0:T(8,128)(2,1)}, u32[]{:S(2)}) copy-start(bf16[2048,256]{1,0:T(8,128)(2,1)} %param.37) | copy-start | bytes 3145732
Sparse Core Ops, SparseCore 0:
  134.4 52.1 all-reduce.2
